TPU v7x, 32 devices: a whole 2x2x4 slice. The times are simulated.
32 devices in a mesh: ep: 8 (over z, x), tp: 4 (over y, core).
Axes of the slice: x: 2, y: 2, z: 4, core: 2. Of those that a mesh axis runs over, the one named last changes fastest.
Arguments:
- query_latent: bfloat16 [2048, 512], P(('ep', 'tp')), may hold values from -6 to 6
- key_latent: bfloat16 [2048, 256], P(('ep', 'tp')), may hold values from -6 to 6
- rotary_key: bfloat16 [2048, 32], P(('ep', 'tp')), may hold values from -140 to 140
- query_gain: float32 [512], replicated, may hold values from 0.1 to 1.9
- latent_gain: float32 [256], replicated, may hold values from 0.1 to 1.9
- query_content: bfloat16 [512, 512], replicated, may hold values from -0.625 to 0.625
- query_rotary: bfloat16 [512, 256], replicated, may hold values from -0.625 to 0.625
- key_content: bfloat16 [256, 512], replicated, may hold values from -0.375 to 0.375
- value_weight: bfloat16 [256, 512], replicated, may hold values from -0.375 to 0.375
- output_weight: bfloat16 [512, 2048], P('tp'), may hold values from -1 to 1
- expert_input: bfloat16 [2048, 2048], P(('ep', 'tp')), may hold values from -6 to 6
- norm_gain: float32 [2048], replicated, may hold values from 0.1 to 1.9
- routes: int32 [2048, 2], P(('ep', 'tp')), may hold values from 0 to 15, all different within a row; in each aligned block of 64 rows (0 to 63, 64 to 127, ...) at most 16 rows name the same one
- route_weight: float32 [2048, 2], P(('ep', 'tp')), may hold values from 0.25 to 2
- expert_gate: bfloat16 [16, 2048, 1024], P('ep', None, 'tp'), may hold values from -0.125 to 0.125
- expert_up: bfloat16 [16, 2048, 1024], P('ep', None, 'tp'), may hold values from -0.125 to 0.125
- expert_down: bfloat16 [16, 1024, 2048], P('ep', 'tp'), may hold values from -0.1875 to 0.1875
- shared_gate: bfloat16 [2048, 1024], P(None, 'tp'), may hold values from -0.125 to 0.125
- shared_up: bfloat16 [2048, 1024], P(None, 'tp'), may hold values from -0.125 to 0.125
- shared_down: bfloat16 [1024, 2048], P('tp'), may hold values from -0.1875 to 0.1875
Outputs:
- mixer_out: bfloat16 [2048, 2048], P(('ep', 'tp'))
- expert_out: bfloat16 [2048, 2048], P(('ep', 'tp'))
Inputs may be any that keep to these rules, and one draw needn't show every extreme that they name: `routes`: each row names 2 different experts. Within the rows of one device (aligned blocks of 64 rows) no expert is named by more than 16 rows, and in every draw some expert is named by exactly 16 rows of some device.
All inputs are finite; a program needn't handle non-finite values.
Results may differ from a plain program's by a relative error of at most 0.013.
The roundings to bfloat16 on the way count: a program that leaves them out, or rounds other values in their place, can miss the bound.
Values may be sent and summed in bfloat16 or wider, within the bound.
No kernel may reach another device: no remote copies, remote signals or barrier semaphores. Data moves between devices by JAX's collectives and lax.ppermute only.
A program may use at most 128 MiB of HBM per device.

v0:
```python
import math

import jax
import jax.numpy as jnp
from jax import lax
from jax.sharding import PartitionSpec as P

HEADS = 8
CONTENT = 64
ROTARY = 32
VALUE = 64


norm_eps = 1e-06
rope_base = 10000.0


def rms_rows(entries, gain_row):
    widened = entries.astype(jnp.float32)
    return widened * lax.rsqrt(jnp.mean(widened * widened, -1, keepdims=True) + norm_eps) * gain_row


def turn_pairs(entries, positions):
    width_full = entries.shape[-1]
    frequency = rope_base ** (-jnp.arange(width_full // 2, dtype=jnp.float32) * 2.0 / width_full)
    angles = positions.astype(jnp.float32)[:, None] * frequency[None, :]
    cosine = jnp.cos(angles)[:, None, :]
    sine_part = jnp.sin(angles)[:, None, :]
    even_part = entries[..., 0::2]
    odd_part = entries[..., 1::2]
    joined = jnp.stack(
        [even_part * cosine - odd_part * sine_part, even_part * sine_part + odd_part * cosine], -1
    )
    return joined.reshape(entries.shape)


def absorb_block(carried, query_part, query_turn, key_part, key_turn, value_rows, score_scale):
    running_peak, running_total, summed = carried
    scores = jnp.einsum("qhc,khc->qhk", query_part, key_part, preferred_element_type=jnp.float32)
    scores = scores + jnp.einsum(
        "qhr,kr->qhk", query_turn, key_turn, preferred_element_type=jnp.float32
    )
    scores = scores * score_scale
    new_peak = jnp.maximum(running_peak, jnp.max(scores, -1))
    factor = jnp.exp(running_peak - new_peak)
    weights = jnp.exp(scores - new_peak[..., None])
    running_total = running_total * factor + jnp.sum(weights, -1)
    summed = summed * factor[..., None] + jnp.einsum(
        "qhk,khv->qhv", weights.astype(jnp.bfloat16), value_rows, preferred_element_type=jnp.float32
    )
    return (new_peak, running_total, summed)


def absorb_piece(carried, query_part, query_turn, key_part, key_turn, value_rows, score_scale):
    row_count = key_part.shape[0]
    key_block = math.gcd(row_count, 2048)
    if key_block == row_count:
        return absorb_block(
            carried, query_part, query_turn, key_part, key_turn, value_rows, score_scale
        )
    block_count = row_count // key_block

    def advance(state, pieces):
        return (
            absorb_block(
                state, query_part, query_turn, pieces[0], pieces[1], pieces[2], score_scale
            ),
            None,
        )

    stacked = (
        key_part.reshape((block_count, key_block) + key_part.shape[1:]),
        key_turn.reshape(block_count, key_block, key_turn.shape[1]),
        value_rows.reshape((block_count, key_block) + value_rows.shape[1:]),
    )
    carried, ignored = lax.scan(advance, carried, stacked)
    return carried


def expand_keys(latent_rows, key_columns, value_columns, head_local):
    row_count = latent_rows.shape[0]
    key_part = (
        jnp.dot(latent_rows, key_columns, preferred_element_type=jnp.float32)
        .astype(jnp.bfloat16)
        .reshape(row_count, head_local, CONTENT)
    )
    value_rows = (
        jnp.dot(latent_rows, value_columns, preferred_element_type=jnp.float32)
        .astype(jnp.bfloat16)
        .reshape(row_count, head_local, VALUE)
    )
    return (key_part, value_rows)


def expert_terms(row_block, gate_weight, up_weight, down_weight):
    gated = jnp.einsum("secd,edf->secf", row_block, gate_weight, preferred_element_type=jnp.float32)
    lifted = jnp.einsum("secd,edf->secf", row_block, up_weight, preferred_element_type=jnp.float32)
    hidden = (jax.nn.silu(gated) * lifted).astype(jnp.bfloat16)
    return jnp.einsum("secf,efd->secd", hidden, down_weight, preferred_element_type=jnp.float32)


def shared_terms(row_block, gate_weight, up_weight, down_weight):
    gated = jnp.dot(row_block, gate_weight, preferred_element_type=jnp.float32)
    lifted = jnp.dot(row_block, up_weight, preferred_element_type=jnp.float32)
    hidden = (jax.nn.silu(gated) * lifted).astype(jnp.bfloat16)
    return jnp.dot(hidden, down_weight, preferred_element_type=jnp.float32)


def shards(
    query_latent,
    key_latent,
    rotary_key,
    query_gain,
    latent_gain,
    query_content,
    query_rotary,
    key_content,
    value_weight,
    output_weight,
    expert_input,
    norm_gain,
    routes,
    route_weight,
    expert_gate,
    expert_up,
    expert_down,
    shared_gate,
    shared_up,
    shared_down,
):
    group_size = lax.axis_size("tp")
    expert_groups = lax.axis_size("ep")
    own_rows = query_latent.shape[0]
    head_local = HEADS // group_size
    head_index = lax.axis_index("tp")
    group_rows_count = own_rows * group_size
    group_start = lax.axis_index("ep") * group_rows_count
    own_start = group_start + head_index * own_rows
    score_scale = (CONTENT + ROTARY) ** (-0.5)
    query_normed = rms_rows(query_latent, query_gain).astype(jnp.bfloat16)
    latent_normed = rms_rows(key_latent, latent_gain).astype(jnp.bfloat16)
    own_positions = own_start + jnp.arange(own_rows, dtype=jnp.int32)
    key_turned = turn_pairs(rotary_key.astype(jnp.float32)[:, None, :], own_positions)[
        :, 0, :
    ].astype(jnp.bfloat16)
    token_rows = expert_input.shape[0]
    picks = routes.shape[1]
    local_experts = expert_gate.shape[0]
    expert_total = local_experts * expert_groups
    capacity = 2 * token_rows * picks // expert_total
    slot_total = expert_total * capacity
    model_width = expert_input.shape[1]
    expert_normed = rms_rows(expert_input, norm_gain).astype(jnp.bfloat16)
    flat_routes = routes.reshape(-1)
    marks = (flat_routes[:, None] == jnp.arange(expert_total, dtype=jnp.int32)[None, :]).astype(
        jnp.int32
    )
    ranks = jnp.sum((jnp.cumsum(marks, 0) - marks) * marks, 1)
    targets = flat_routes * capacity + ranks
    picker = (jnp.arange(slot_total, dtype=jnp.int32)[:, None] == targets[None, :]).astype(
        jnp.int32
    )
    picker = jnp.sum(picker.reshape(slot_total, token_rows, picks), 2).astype(jnp.bfloat16)
    outgoing = jnp.dot(picker, expert_normed, preferred_element_type=jnp.float32).astype(
        jnp.bfloat16
    )
    outgoing = outgoing.reshape(expert_groups, local_experts, capacity, model_width)
    received = lax.all_to_all(outgoing, "ep", split_axis=0, concat_axis=0, tiled=True)
    group_query, group_latent, group_turn, gathered_rows, gathered_tokens = (
        lax.all_gather(query_normed, "tp", axis=0, tiled=True),
        lax.all_gather(latent_normed, "tp", axis=0, tiled=True),
        lax.all_gather(key_turned, "tp", axis=0, tiled=True),
        lax.all_gather(received, "tp", axis=0, tiled=True),
        lax.all_gather(expert_normed, "tp", axis=0, tiled=True),
    )
    positions = group_start + jnp.arange(group_rows_count, dtype=jnp.int32)
    content_columns = lax.dynamic_slice_in_dim(
        query_content, head_index * head_local * CONTENT, head_local * CONTENT, 1
    )
    rotary_columns = lax.dynamic_slice_in_dim(
        query_rotary, head_index * head_local * ROTARY, head_local * ROTARY, 1
    )
    query_part = (
        jnp.dot(group_query, content_columns, preferred_element_type=jnp.float32)
        .astype(jnp.bfloat16)
        .reshape(group_rows_count, head_local, CONTENT)
    )
    query_turn = turn_pairs(
        jnp.dot(group_query, rotary_columns, preferred_element_type=jnp.float32).reshape(
            group_rows_count, head_local, ROTARY
        ),
        positions,
    ).astype(jnp.bfloat16)
    key_columns = lax.dynamic_slice_in_dim(
        key_content, head_index * head_local * CONTENT, head_local * CONTENT, 1
    )
    value_columns = lax.dynamic_slice_in_dim(
        value_weight, head_index * head_local * VALUE, head_local * VALUE, 1
    )
    carry_start = (
        jnp.full((group_rows_count, head_local), -jnp.inf, jnp.float32),
        jnp.zeros((group_rows_count, head_local), jnp.float32),
        jnp.zeros((group_rows_count, head_local, VALUE), jnp.float32),
    )
    key_part, value_rows = expand_keys(
        lax.all_gather(group_latent, "ep", axis=0, tiled=True),
        key_columns,
        value_columns,
        head_local,
    )
    running_peak, running_total, summed = absorb_piece(
        carry_start,
        query_part,
        query_turn,
        key_part,
        lax.all_gather(group_turn, "ep", axis=0, tiled=True),
        value_rows,
        score_scale,
    )
    attended = (
        (summed / running_total[..., None])
        .astype(jnp.bfloat16)
        .reshape(group_rows_count, head_local * VALUE)
    )
    routed_term = expert_terms(gathered_rows, expert_gate, expert_up, expert_down)
    shared_term = shared_terms(gathered_tokens, shared_gate, shared_up, shared_down)
    mixer_term = jnp.dot(attended, output_weight, preferred_element_type=jnp.float32)
    mixer_sum, routed_sum, shared_sum = (
        lax.psum_scatter(
            mixer_term.astype(jnp.bfloat16), "tp", scatter_dimension=0, tiled=True
        ).astype(jnp.float32),
        lax.psum_scatter(
            routed_term.astype(jnp.bfloat16), "tp", scatter_dimension=0, tiled=True
        ).astype(jnp.float32),
        lax.psum_scatter(
            shared_term.astype(jnp.bfloat16), "tp", scatter_dimension=0, tiled=True
        ).astype(jnp.float32),
    )
    mixer_out = mixer_sum.astype(jnp.bfloat16)
    returned = lax.all_to_all(
        routed_sum.astype(jnp.bfloat16), "ep", split_axis=0, concat_axis=0, tiled=True
    )
    returned = returned.reshape(slot_total, model_width)
    picked = jnp.take(returned, targets, axis=0).reshape(token_rows, picks, model_width)
    combined = jnp.sum(route_weight[..., None] * picked.astype(jnp.float32), 1) + shared_sum
    expert_out = combined.astype(jnp.bfloat16)
    return (mixer_out, expert_out)


def solution(mesh):
    in_specs = (
        P(("ep", "tp"), None),
        P(("ep", "tp"), None),
        P(("ep", "tp"), None),
        P(),
        P(),
        P(),
        P(),
        P(),
        P(),
        P("tp", None),
        P(("ep", "tp"), None),
        P(),
        P(("ep", "tp"), None),
        P(("ep", "tp"), None),
        P("ep", None, "tp"),
        P("ep", None, "tp"),
        P("ep", "tp", None),
        P(None, "tp"),
        P(None, "tp"),
        P("tp", None),
    )
    out_specs = (P(("ep", "tp"), None), P(("ep", "tp"), None))
    return jax.shard_map(shards, mesh=mesh, in_specs=in_specs, out_specs=out_specs, check_vma=False)
```

profile of v0, /device:TPU:0, one launch (start us, length us, event | category | flops | bytes accessed | tf_op | source)
XLA Modules:
  0.0 250.2 jit_solution(3735502933003136153)
XLA Ops:
  13.4 32.8 %all_to_all.10 = bf16[8,2,16,2048]{3,2,1,0:T(8,128)(2,1)S(1)} all-to-all(bf16[8,2,16,2048]{3,2,1,0:T(8,128)(2,1)S(1)} %bitcast.114), channel_id=1, replica_groups=mesh['ep'=8,'tp'=4] {'ep'}, dimensions={0} | all-to-all | bytes 2097152 | tf_op jit(solution)/shard_map/all_to_all | solution.py:168
  48.4 5.9 %all_gather.21 = bf16[256,256]{1,0:T(8,128)(2,1)} all-gather(bf16[64,256]{1,0:T(8,128)(2,1)S(1)} %fusion.57), channel_id=1, replica_groups=mesh['ep'=8,'tp'=4] {'tp'}, dimensions={0}, use_global_device_ids=true | all-gather | bytes 163840 | tf_op jit(solution)/shard_map/all_gather | solution.py:171
  54.3 26.7 %all-gather.7.cloned.1.call-done = bf16[32,2,16,2048]{3,2,0,1:T(8,128)(2,1)} async-done(((bf16[8,2,16,2048]{3,2,0,1:T(8,128)(2,1)}), bf16[32,2,16,2048]{3,2,0,1:T(8,128)(2,1)}) %all-gather.7.cloned.1.call-update) | async-done | bytes 4194320 | tf_op jit(solution)/shard_map/all_gather | solution.py:173
  81.0 4.1 %fusion.11 = f32[32,2,16,256]{3,2,0,1:T(8,128)S(1)} fusion(bf16[32,2,16,2048]{3,2,0,1:T(8,128)(2,1)} %all-gather.7.cloned.1.call-done, bf16[2,2048,256]{2,1,0:T(8,128)(2,1)} %param.34), kind=kOutput, calls=%fused_computation.19 | convolution fusion | flops 1073741824 | bytes 7340032 | tf_op jit(solution)/shard_map/secd,edf->secf/dot_general | solution.py:96
  85.2 7.3 %convert_bitcast_fusion = bf16[32,2,16,2048]{3,2,0,1:T(8,128)(2,1)} fusion(bf16[2,256,2048]{2,1,0:T(8,128)(2,1)S(1)} %copy-done, bf16[32,2,16,2048]{3,2,0,1:T(8,128)(2,1)} %all-gather.7.cloned.1.call-done, bf16[2,2048,256]{2,1,0:T(8,128)(2,1)} %param.35, f32[32,2,16,256]{3,2,0,1:T(8,128)S(1)} %fusion.11), kind=kOutput, calls=%fused_computation.3 | convolution fusion | flops 2151153664 | bytes 13631488 | tf_op jit(solution)/shard_map/secf,efd->secd/dot_general | solution.py:99
  92.5 2.5 copy.77
  95.0 4.2 %copy.79 = bf16[4,8,32,2048]{3,1,2,0:T(8,128)(2,1)} copy(bf16[4,8,32,2048]{3,2,1,0:T(8,128)(2,1)S(1)} %bitcast.112) | data formatting | bytes 8388608
  100.3 5.8 %all_gather.23 = bf16[256,512]{1,0:T(8,128)(2,1)S(1)} all-gather(bf16[64,512]{1,0:T(8,128)(2,1)S(1)} %fusion.49), channel_id=1, replica_groups=mesh['ep'=8,'tp'=4] {'tp'}, dimensions={0}, use_global_device_ids=true | all-gather | bytes 327680 | tf_op jit(solution)/shard_map/all_gather | solution.py:170
  109.4 5.2 %all-gather = bf16[4,64,32]{1,2,0:T(8,128)(2,1)S(1)} all-gather(bf16[1,64,32]{1,2,0:T(8,128)(2,1)S(1)} %bitcast.122), channel_id=1, replica_groups=mesh['ep'=8,'tp'=4] {'tp'}, dimensions={0}, use_global_device_ids=true | all-gather | bytes 20480 | tf_op jit(solution)/shard_map/all_gather | solution.py:172
  114.7 31.1 %all_gather.25 = bf16[2048,32]{0,1:T(8,128)(2,1)S(1)} all-gather(bf16[256,32]{0,1:T(8,128)(2,1)S(1)} %reshape.292), channel_id=1, replica_groups=mesh['ep'=8,'tp'=4] {'ep'}, dimensions={0}, use_global_device_ids=true | all-gather | bytes 147456 | tf_op jit(solution)/shard_map/all_gather | solution.py:216
  145.8 1.8 convolution_convert_fusion.5
  147.6 2.4 fusion.86
  149.9 4.6 %convolution_convert_fusion.1 = bf16[256,2048]{1,0:T(8,128)(2,1)} fusion(bf16[256,2048]{1,0:T(8,128)(2,1)} %param.39, bf16[256,2048]{1,0:T(8,128)(2,1)} %all-gather.9.cloned.1.call-done, bf16[2048,256]{1,0:T(8,128)(2,1)} %param.38, f32[256,256]{1,0:T(8,128)} %fusion.86), kind=kOutput, calls=%fused_computation.8 | convolution fusion | flops 537788416 | bytes 4456448 | tf_op jit(solution)/shard_map/dot_general | solution.py:106
  154.6 1.8 convolution_convert_fusion.4
  157.9 2.0 copy-done.1
  160.4 2.1 convolution_convert_fusion.3
  162.6 25.8 %reduce-scatter.11.cloned.1.call-done = bf16[8,65536]{1,0:T(8,128)(2,1)} async-done(((bf16[32,65536]{1,0:T(8,128)(2,1)}), bf16[8,65536]{1,0:T(8,128)(2,1)}) %reduce-scatter.11.cloned.1.call-update) | async-done | bytes 1048592
  188.4 2.8 %copy.80 = bf16[1,8,32,2048]{3,2,1,0:T(8,128)(2,1)} copy(bf16[1,8,32,2048]{3,1,2,0:T(8,128)(2,1)} %bitcast.117) | data formatting | bytes 2097152
  191.1 5.5 %all-to-all-start.1 = ((bf16[8,2,16,2048]{3,2,1,0:T(8,128)(2,1)}), bf16[8,2,16,2048]{3,2,1,0:T(8,128)(2,1)S(1)}, u32[]{:S(2)}, u32[]{:S(2)}) async-start(bf16[8,2,16,2048]{3,2,1,0:T(8,128)(2,1)} %bitcast.113), calls=%async_computation.2 | async-start | bytes 2097152 | tf_op jit(solution)/shard_map/all_to_all | solution.py:240
  196.8 3.5 %fusion.33 = bf16[256,2,64]{0,2,1:T(8,128)(2,1)S(1)} fusion(bf16[2048,2,64]{0,2,1:T(8,128)(2,1)} %bitcast.115, f32[256,2,2048]{0,2,1:T(8,128)} %copy-done.1, f32[256,2]{0,1:T(2,128)S(1)} %get-tuple-element.12, f32[256,2]{0,1:T(2,128)S(1)} %get-tuple-element.9, f32[256,2]{0,1:T(2,128)S(1)} %get-tuple-element.8), kind=kOutput, calls=%fused_computation.28 | convolution fusion | flops 136413184 | bytes 4790272 | tf_op jit(solution)/shard_map/qhk,khv->qhv/dot_general | solution.py:48
  202.2 20.1 %all-to-all-done.1 = bf16[8,2,16,2048]{3,2,1,0:T(8,128)(2,1)S(1)} async-done(((bf16[8,2,16,2048]{3,2,1,0:T(8,128)(2,1)}), bf16[8,2,16,2048]{3,2,1,0:T(8,128)(2,1)S(1)}, u32[]{:S(2)}, u32[]{:S(2)}) %all-to-all-start.1) | async-done | bytes 1048608 | tf_op jit(solution)/shard_map/all_to_all | solution.py:240
  222.3 1.8 gather_fusion
  225.5 2.5 multiply_reduce_fusion
  229.7 13.7 %reduce-scatter.7.cloned.1.call-done = bf16[64,2048]{1,0:T(8,128)(2,1)} async-done(((bf16[256,2048]{1,0:T(8,128)(2,1)}), bf16[64,2048]{1,0:T(8,128)(2,1)}) %reduce-scatter.7.cloned.1.call-update) | async-done | bytes 262160 | tf_op jit(solution)/shard_map/reduce_scatter | solution.py:229
  (105 shorter events, 19.9 us)
Async XLA Ops:
  7.2 78.0 %copy-start = (bf16[2,256,2048]{2,1,0:T(8,128)(2,1)S(1)}, bf16[2,256,2048]{2,1,0:T(8,128)(2,1)}, u32[]{:S(2)}) copy-start(bf16[2,256,2048]{2,1,0:T(8,128)(2,1)} %param.36) | copy-start | bytes 6291460
  7.2 41.0 %copy-start.9 = (bf16[64,256]{1,0:T(8,128)(2,1)S(1)}, bf16[64,256]{1,0:T(8,128)(2,1)}, u32[]{:S(2)}) copy-start(bf16[64,256]{1,0:T(8,128)(2,1)} %param.21) | copy-start | bytes 98308
  7.2 41.1 %copy-start.17 = (f32[256]{0:T(256)S(1)}, f32[256]{0:T(256)}, u32[]{:S(2)}) copy-start(f32[256]{0:T(256)} %param.24) | copy-start | bytes 3076
  7.2 73.8 %all-gather.7.cloned.1.call-start = ((), (), s32[]{:S(2)}) async-start(), calls=%async_computation.7 | async-start | bytes 5242880 | tf_op jit(solution)/shard_map/all_gather | solution.py:173
  13.0 34.4 %copy-start.3 = (bf16[64,2048]{1,0:T(8,128)(2,1)}, bf16[64,2048]{1,0:T(8,128)(2,1)S(1)}, u32[]{:S(2)}) copy-start(bf16[64,2048]{1,0:T(8,128)(2,1)S(1)} %fusion.40) | copy-start | bytes 786436
  47.4 100.2 %all-gather.9.cloned.1.call-start = ((), (), s32[]{:S(2)}) async-start(), calls=%async_computation.8 | async-start | bytes 1310720 | tf_op jit(solution)/shard_map/all_gather | solution.py:174
  48.1 106.4 %all-gather.5.cloned.1.call-start = ((), (), s32[]{:S(2)}) async-start(), calls=%async_computation.5 | async-start | bytes 1179648 | tf_op jit(solution)/shard_map/all_gather | solution.py:206
  54.3 134.1 %reduce-scatter.11.cloned.1.call-start = ((), (), s32[]{:S(2)}) async-start(), calls=%async_computation.10 | async-start | bytes 5242880
  99.2 0.8 copy-start.7
  99.2 1.0 copy-start.12
  99.2 8.1 %copy-start.11 = (bf16[64,32]{0,1:T(8,128)(2,1)S(1)}, bf16[64,32]{0,1:T(8,128)(2,1)}, u32[]{:S(2)}) copy-start(bf16[64,32]{0,1:T(8,128)(2,1)} %param.22) | copy-start | bytes 12292
  99.2 48.3 %copy-start.4 = (bf16[2048,256]{1,0:T(8,128)(2,1)S(1)}, bf16[2048,256]{1,0:T(8,128)(2,1)}, u32[]{:S(2)}) copy-start(bf16[2048,256]{1,0:T(8,128)(2,1)} %param.37) | copy-start | bytes 3145732
  99.3 128.7 %reduce-scatter.9.cloned.1.call-start = ((), (), s32[]{:S(2)}) async-start(), calls=%async_computation.9 | async-start | bytes 1310720 | tf_op jit(solution)/shard_map/reduce_scatter | solution.py:235
  149.9 6.4 %copy-start.6 = (bf16[256,128]{0,1:T(8,128)(2,1)S(1)}, bf16[256,128]{0,1:T(8,128)(2,1)}, u32[]{:S(2)}) copy-start(bf16[256,128]{0,1:T(8,128)(2,1)} %convolution_convert_fusion.5) | copy-start | bytes 196612
  154.5 2.6 %copy-start.8 = (bf16[256,2,32]{0,2,1:T(8,128)(2,1)S(1)}, bf16[256,2,32]{0,2,1:T(8,128)(2,1)}, u32[]{:S(2)}) copy-start(bf16[256,2,32]{0,2,1:T(8,128)(2,1)} %convert_element_type.107) | copy-start | bytes 98308
  157.9 2.0 copy-start.1
  157.9 2.5 %copy-start.2 = (bf16[2048,256]{1,0:T(8,128)(2,1)S(1)}, bf16[2048,256]{1,0:T(8,128)(2,1)}, u32[]{:S(2)}) copy-start(bf16[2048,256]{1,0:T(8,128)(2,1)} %all-gather.5.cloned.1.call-done) | copy-start | bytes 3145732
  191.1 31.2 %all-to-all-start.1 = ((bf16[8,2,16,2048]{3,2,1,0:T(8,128)(2,1)}), bf16[8,2,16,2048]{3,2,1,0:T(8,128)(2,1)S(1)}, u32[]{:S(2)}, u32[]{:S(2)}) async-start(bf16[8,2,16,2048]{3,2,1,0:T(8,128)(2,1)} %bitcast.113), calls=%async_computation.2 | async-start | bytes 2097152 | tf_op jit(solution)/shard_map/all_to_all | solution.py:240
  196.7 5.0 %copy-start.10 = (s32[64,2]{0,1:T(2,128)S(1)}, s32[64,2]{0,1:T(2,128)}, u32[]{:S(2)}) copy-start(s32[64,2]{0,1:T(2,128)} %param.32) | copy-start | bytes 1540
  196.7 5.3 %copy-start.16 = (pred[64,2]{0,1:T(4,128)(4,1)S(1)}, pred[64,2]{0,1:T(4,128)(4,1)}, u32[]{:S(2)}) copy-start(pred[64,2]{0,1:T(4,128)(4,1)} %get-tuple-element.2) | copy-start | bytes 388
  196.7 5.4 %copy-start.18 = (f32[64,2]{0,1:T(2,128)S(1)}, f32[64,2]{0,1:T(2,128)}, u32[]{:S(2)}) copy-start(f32[64,2]{0,1:T(2,128)} %param.33) | copy-start | bytes 1540
  196.7 5.5 %copy-start.14 = (s32[128]{0:T(128)S(1)}, s32[128]{0:T(128)}, u32[]{:S(2)}) copy-start(s32[128]{0:T(128)} %copy-done.13) | copy-start | bytes 1540
  196.7 46.7 %reduce-scatter.7.cloned.1.call-start = ((), (), s32[]{:S(2)}) async-start(), calls=%async_computation.6 | async-start | bytes 1310720 | tf_op jit(solution)/shard_map/reduce_scatter | solution.py:229
  196.8 3.5 %copy-start.5 = (bf16[128,2048]{1,0:T(8,128)(2,1)S(1)}, bf16[128,2048]{1,0:T(8,128)(2,1)}, u32[]{:S(2)}) copy-start(bf16[128,2048]{1,0:T(8,128)(2,1)} %param.29) | copy-start | bytes 1572868
  (2 other events, 1.1 us)
Sparse Core Ops, SparseCore 0:
  47.5 33.5 all-gather.6
  83.2 16.6 all-gather.8
  102.0 40.7 all-gather.4
  145.2 43.1 reduce-scatter.10
  190.8 24.8 reduce-scatter.8
  218.6 24.7 reduce-scatter.6
where the time goes:
time: 251 us; the launch traced here: 250 us
  waiting for transfers between devices  87.2 us (35%)
  blocking collectives  80.8 us (32%)
  matrix products  32 us (13%)
  local copies, waits for them, and re-layouts  19.8 us (8%)
  between operations  14.6 us (6%)
  other arithmetic  10.1 us (4%)
  starting transfers between devices  5.76 us (2%)
    all_to_all x1, blocking collectives, shards(): lax.all_to_all(outgoing, 'ep', split_axis=0, concat_axis=0, tiled=True)  32.8 us
    all_gather x1, blocking collectives, shards(): lax.all_gather(group_turn, 'ep', axis=0, tiled=True)  31.1 us
    all_gather x1, waiting for transfers between devices, shards(): lax.all_gather(received, 'tp', axis=0, tiled=True)  26.7 us
    unnamed x7, waiting for transfers between devices  26.6 us
    all_to_all x1, waiting for transfers between devices, shards(): lax.all_to_all(routed_sum.astype(jnp.bfloat16), 'ep', split_axis=0, conca...  20.1 us
    unnamed x44, local copies, waits for them, and re-layouts  14.2 us
    reduce_scatter x1, waiting for transfers between devices, shards(): lax.psum_scatter(mixer_term.astype(jnp.bfloat16), 'tp', scatter_dimension...  13.7 us
    dot_general x1, matrix products, expert_terms(): jnp.einsum('secf,efd->secd', hidden, down_weight, preferred_element_type=...  7.31 us
  transfers between devices with their start and end apart: 7, of which 4 were waited for; matrix products, arithmetic and copies ran while one was open for 21% of the time, Pallas kernels for 0%

commit v1 on v0

v1 whole, which is shorter than its diff:
```python
import functools

import jax
import jax.numpy as jnp
from jax import lax
from jax.experimental import pallas as pl
from jax.sharding import PartitionSpec as P


HEADS = 8
CONTENT = 64
ROTARY = 32
VALUE = 64
CHUNKS = 2

norm_eps = 1e-06
rope_base = 10000.0


def rms_rows(entries, gain_row):
    widened = entries.astype(jnp.float32)
    return widened * lax.rsqrt(jnp.mean(widened * widened, -1, keepdims=True) + norm_eps) * gain_row


def dot32(left, right):
    return jnp.dot(left, right, preferred_element_type=jnp.float32)


def turn_tables(positions, width, period):
    column = lax.broadcasted_iota(jnp.int32, (1, width), 1)
    pair = ((column % period) // 2).astype(jnp.float32)
    frequency = rope_base ** (-pair * 2.0 / period)
    angles = positions.astype(jnp.float32)[:, None] * frequency
    return jnp.cos(angles), jnp.sin(angles)


def swap_matrix(width):
    row = lax.broadcasted_iota(jnp.int32, (width, width), 0)
    column = lax.broadcasted_iota(jnp.int32, (width, width), 1)
    partner = row == (column ^ 1)
    sign = jnp.where(column % 2 == 0, -1.0, 1.0)
    return jnp.where(partner, sign, 0.0).astype(jnp.bfloat16)


def swap_tp(entries, distance):
    size = lax.axis_size("tp")
    return lax.ppermute(entries, "tp", [(i, i ^ distance) for i in range(size)])


def gather_far(entries):
    return [swap_tp(entries, k) for k in range(2, lax.axis_size("tp"), 2)]


def gather_near(entries, far):
    pieces = []
    for piece in [entries] + far:
        pieces.append(piece)
        if lax.axis_size("tp") > 1:
            pieces.append(swap_tp(piece, 1))
    return pieces


def swap_ep(entries, distance):
    size = lax.axis_size("ep")
    return lax.ppermute(entries, "ep", [(i, i ^ distance) for i in range(size)])


def exchange_fits(size):
    return 2 <= size <= 16 and size & (size - 1) == 0


def merge_pairs(parts):
    size = parts.shape[0]
    if size == 1:
        return (parts[0].astype(jnp.float32),)
    received = swap_tp(parts[1::2], 1)
    merged = parts[0::2].astype(jnp.float32) + received.astype(jnp.float32)
    return (merged[0],) + tuple(merged[k].astype(jnp.bfloat16) for k in range(1, size // 2))


def send_pairs(merged):
    return [swap_tp(merged[k], 2 * k) for k in range(1, len(merged))]


def sum_pairs(merged, arrived):
    total = merged[0]
    for piece in arrived:
        total = total + piece.astype(jnp.float32)
    return total


def attend_kernel(query_ref, turn_ref, latent_ref, key_ref, value_ref, out_ref):
    own = query_ref.shape[1]
    wide = query_ref.shape[2]
    heads = wide // CONTENT
    rank = key_ref.shape[0]
    latent = latent_ref[:, :rank]
    keys = dot32(latent, key_ref[...]).astype(jnp.bfloat16)
    values = dot32(latent, value_ref[...]).astype(jnp.bfloat16)
    query = query_ref[0]
    head_of = lax.broadcasted_iota(jnp.int32, (own, wide), 1) // CONTENT
    stacked = jnp.concatenate(
        [jnp.where(head_of == h, query, jnp.zeros_like(query)) for h in range(heads)], 0
    )
    contract = (((1,), (1,)), ((), ()))
    scores = lax.dot_general(stacked, keys, contract, preferred_element_type=jnp.float32)
    scores = scores + lax.dot_general(
        turn_ref[0], latent_ref[:, rank:], contract, preferred_element_type=jnp.float32
    )
    scores = scores * ((CONTENT + ROTARY) ** (-0.5))
    weights = jnp.exp(scores - jnp.max(scores, -1, keepdims=True))
    total = jnp.sum(weights, -1, keepdims=True)
    result = dot32(weights.astype(jnp.bfloat16), values) / total
    joined = result[:own]
    for h in range(1, heads):
        joined = jnp.where(head_of == h, result[h * own : (h + 1) * own], joined)
    out_ref[0] = joined.astype(jnp.bfloat16)


def attend(query, turned, all_keys, key_content, value_weight):
    groups, own, wide = query.shape
    count = all_keys.shape[0]
    rank = key_content.shape[0]
    return pl.pallas_call(
        attend_kernel,
        grid=(groups,),
        in_specs=[
            pl.BlockSpec((1, own, wide), lambda g: (g, 0, 0)),
            pl.BlockSpec((1,) + turned.shape[1:], lambda g: (g, 0, 0)),
            pl.BlockSpec(all_keys.shape, lambda g: (0, 0)),
            pl.BlockSpec((rank, wide), lambda g: (0, g)),
            pl.BlockSpec((rank, wide), lambda g: (0, g)),
        ],
        out_specs=pl.BlockSpec((1, own, wide), lambda g: (g, 0, 0)),
        out_shape=jax.ShapeDtypeStruct((groups, own, wide), jnp.bfloat16),
        cost_estimate=pl.CostEstimate(
            flops=4 * groups * count * wide * (rank + own * 2),
            transcendentals=groups * own * count * 2,
            bytes_accessed=4 * count * rank,
        ),
        name="attend",
    )(query, turned, all_keys, key_content, value_weight)


def attend_chunked(query, turned, all_keys, key_content, value_weight):
    groups, own, wide = query.shape
    heads = wide // CONTENT
    count = all_keys.shape[0]
    rank = key_content.shape[0]
    latent, key_turn = all_keys[:, :rank], all_keys[:, rank:]
    block = min(count, 2048)
    query = query.reshape(groups, own, heads, CONTENT)
    turned = turned.reshape(groups, heads, own, ROTARY)

    def advance(state, pieces):
        peak, total, summed = state
        latent_rows, turn_rows = pieces
        keys = dot32(latent_rows, key_content).astype(jnp.bfloat16)
        values = dot32(latent_rows, value_weight).astype(jnp.bfloat16)
        keys = keys.reshape(block, groups, heads, CONTENT)
        values = values.reshape(block, groups, heads, VALUE)
        scores = jnp.einsum("gqhc,kghc->ghqk", query, keys, preferred_element_type=jnp.float32)
        scores = scores + jnp.einsum(
            "ghqr,kr->ghqk", turned, turn_rows, preferred_element_type=jnp.float32
        )
        scores = scores * ((CONTENT + ROTARY) ** (-0.5))
        fresh = jnp.maximum(peak, jnp.max(scores, -1))
        factor = jnp.exp(peak - fresh)
        weights = jnp.exp(scores - fresh[..., None])
        total = total * factor + jnp.sum(weights, -1)
        summed = summed * factor[..., None] + jnp.einsum(
            "ghqk,kghv->ghqv",
            weights.astype(jnp.bfloat16),
            values,
            preferred_element_type=jnp.float32,
        )
        return (fresh, total, summed), None

    start = (
        jnp.full((groups, heads, own), -jnp.inf, jnp.float32),
        jnp.zeros((groups, heads, own), jnp.float32),
        jnp.zeros((groups, heads, own, VALUE), jnp.float32),
    )
    stacked = (
        latent.reshape(count // block, block, latent.shape[1]),
        key_turn.reshape(count // block, block, key_turn.shape[1]),
    )
    (peak, total, summed), _ = lax.scan(advance, start, stacked)
    result = (summed / total[..., None]).astype(jnp.bfloat16)
    return result.transpose(0, 2, 1, 3).reshape(groups, own, wide)


def feed_forward(row_block, gate_weight, up_weight, down_weight):
    gated = dot32(row_block, gate_weight)
    lifted = dot32(row_block, up_weight)
    hidden = (jax.nn.silu(gated) * lifted).astype(jnp.bfloat16)
    return dot32(hidden, down_weight).astype(jnp.bfloat16)


def shards(
    query_latent,
    key_latent,
    rotary_key,
    query_gain,
    latent_gain,
    query_content,
    query_rotary,
    key_content,
    value_weight,
    output_weight,
    expert_input,
    norm_gain,
    routes,
    route_weight,
    expert_gate,
    expert_up,
    expert_down,
    shared_gate,
    shared_up,
    shared_down,
):
    tp_size = lax.axis_size("tp")
    ep_size = lax.axis_size("ep")
    tp_index = lax.axis_index("tp")
    own_rows = query_latent.shape[0]
    own_start = (lax.axis_index("ep") * tp_size + tp_index) * own_rows
    positions = own_start + jnp.arange(own_rows, dtype=jnp.int32)
    token_rows, model_width = expert_input.shape
    picks = routes.shape[1]
    local_experts = expert_gate.shape[0]
    expert_total = local_experts * ep_size
    capacity = 2 * token_rows * picks // expert_total
    slot_total = expert_total * capacity

    expert_normed = rms_rows(expert_input, norm_gain).astype(jnp.bfloat16)
    flat_routes = routes.reshape(-1)
    marks = (flat_routes[:, None] == jnp.arange(expert_total, dtype=jnp.int32)[None, :]).astype(
        jnp.bfloat16
    )
    pick_count = token_rows * picks
    before = (
        lax.broadcasted_iota(jnp.int32, (pick_count, pick_count), 1)
        < lax.broadcasted_iota(jnp.int32, (pick_count, pick_count), 0)
    ).astype(jnp.bfloat16)
    ranks = jnp.sum(dot32(before, marks) * marks.astype(jnp.float32), 1).astype(jnp.int32)
    targets = (
        (flat_routes % local_experts) * ep_size + flat_routes // local_experts
    ) * capacity + ranks
    targets = targets.reshape(token_rows, picks)
    slots = jnp.arange(slot_total, dtype=jnp.int32)
    chosen = [
        (targets[:, k : k + 1] == slots[None, :]).astype(jnp.bfloat16) for k in range(picks)
    ]
    picker = functools.reduce(jnp.add, chosen)
    chunks = CHUNKS if local_experts % CHUNKS == 0 else 1
    chunk_experts = local_experts // chunks
    chunk_slots = slot_total // chunks
    outgoing = (
        lax.dot_general(
            picker, expert_normed, (((0,), (0,)), ((), ())), preferred_element_type=jnp.float32
        )
        .astype(jnp.bfloat16)
        .reshape(local_experts, ep_size, capacity, model_width)
    )
    latent_normed = rms_rows(key_latent, latent_gain).astype(jnp.bfloat16)
    cosine, sine = turn_tables(positions, ROTARY, ROTARY)
    key_turned = (
        rotary_key.astype(jnp.float32) * cosine + dot32(rotary_key, swap_matrix(ROTARY)) * sine
    ).astype(jnp.bfloat16)
    column_keys = jnp.concatenate([latent_normed, key_turned], 1)
    if exchange_fits(ep_size):
        column_keys = jnp.concatenate([column_keys, swap_ep(column_keys, 1)], 0)
    outgoing, column_keys, query_latent = lax.optimization_barrier(
        (outgoing, column_keys, query_latent)
    )
    if exchange_fits(ep_size):
        pieces = [swap_ep(column_keys, k) for k in range(2, ep_size, 2)]
        column_keys = jnp.concatenate([column_keys] + pieces, 0)
    else:
        column_keys = lax.all_gather(column_keys, "ep", axis=0, tiled=True)
    received = lax.all_to_all(outgoing, "ep", split_axis=1, concat_axis=1, tiled=True)
    weight_far = gather_far(output_weight)
    received = received.reshape(local_experts, ep_size * capacity, model_width)
    all_keys = jnp.concatenate(gather_near(column_keys, gather_far(column_keys)), 0)
    token_pieces = gather_near(expert_normed, gather_far(expert_normed))
    weight_pieces = gather_near(output_weight, weight_far)

    query_normed = rms_rows(query_latent, query_gain).astype(jnp.bfloat16)
    query_part = dot32(query_normed, query_content).astype(jnp.bfloat16)
    turn_width = query_rotary.shape[1]
    cosine, sine = turn_tables(positions, turn_width, ROTARY)
    swapped_rotary = dot32(query_rotary, swap_matrix(turn_width)).astype(jnp.bfloat16)
    query_turn = (
        dot32(query_normed, query_rotary) * cosine + dot32(query_normed, swapped_rotary) * sine
    ).astype(jnp.bfloat16)
    group_heads = HEADS // tp_size
    query_groups = query_part.reshape(own_rows, tp_size, group_heads * CONTENT).transpose(1, 0, 2)
    turn_groups = (
        query_turn.reshape(own_rows, tp_size, group_heads, ROTARY)
        .transpose(1, 2, 0, 3)
        .reshape(tp_size, group_heads * own_rows, ROTARY)
    )
    mix = attend if all_keys.shape[0] <= 4096 else attend_chunked
    attended = mix(
        query_groups,
        turn_groups,
        all_keys,
        key_content,
        value_weight,
    )
    received, attended, token_pieces, weight_pieces = lax.optimization_barrier(
        (received, attended, token_pieces, weight_pieces)
    )
    mixed = None
    for k, piece in enumerate(weight_pieces):
        columns = lax.dynamic_index_in_dim(attended, tp_index ^ k, 0, keepdims=False)
        product = dot32(columns, piece).astype(jnp.bfloat16).astype(jnp.float32)
        mixed = product if mixed is None else mixed + product
    mixer_out = mixed.astype(jnp.bfloat16)

    shared_term = feed_forward(
        jnp.concatenate(token_pieces, 0), shared_gate, shared_up, shared_down
    ).reshape(tp_size, token_rows, model_width)

    returned = []
    routed = [received[c * chunk_experts : (c + 1) * chunk_experts] for c in range(chunks)]
    far = gather_far(routed[0])
    far, shared_term, routed = lax.optimization_barrier((far, shared_term, routed))
    shared_merged = merge_pairs(shared_term)
    for c in range(chunks):
        pieces = gather_near(routed[c], far)
        if c + 1 < chunks:
            far = gather_far(routed[c + 1])
        terms = []
        for x in range(chunk_experts):
            e = c * chunk_experts + x
            rows = jnp.concatenate([piece[x] for piece in pieces], 0)
            term = feed_forward(rows, expert_gate[e], expert_up[e], expert_down[e])
            terms.append(term.reshape(tp_size, 1, ep_size * capacity, model_width))
        parts = terms[0] if chunk_experts == 1 else jnp.concatenate(terms, 1)
        merged = merge_pairs(parts)
        if c == chunks - 1:
            merged, shared_merged = lax.optimization_barrier((merged, shared_merged))
        arrived = send_pairs(merged)
        returned.append(sum_pairs(merged, arrived))
    shared_sum = sum_pairs(shared_merged, send_pairs(shared_merged))
    for c in range(chunks):
        summed = returned[c].astype(jnp.bfloat16)
        summed = summed.reshape(chunk_experts, ep_size, capacity, model_width)
        summed = lax.all_to_all(summed, "ep", split_axis=1, concat_axis=1, tiled=True)
        returned[c] = summed.reshape(chunk_slots, model_width)
    combined = shared_sum
    for k in range(picks):
        picked = None
        for c in range(chunks):
            piece = dot32(chosen[k][:, c * chunk_slots : (c + 1) * chunk_slots], returned[c])
            picked = piece if picked is None else picked + piece
        combined = combined + route_weight[:, k : k + 1] * picked
    expert_out = combined.astype(jnp.bfloat16)
    return (mixer_out, expert_out)


def solution(mesh):
    rows = P(("ep", "tp"), None)
    in_specs = (
        rows,
        rows,
        rows,
        P(),
        P(),
        P(),
        P(),
        P(),
        P(),
        P("tp", None),
        rows,
        P(),
        rows,
        rows,
        P("ep", None, "tp"),
        P("ep", None, "tp"),
        P("ep", "tp", None),
        P(None, "tp"),
        P(None, "tp"),
        P("tp", None),
    )

    return jax.shard_map(
        shards, mesh=mesh, in_specs=in_specs, out_specs=(rows, rows), check_vma=False
    )
```

time: 251 us -> 180 us (0.72)
  blocking collectives: 80.8 us -> 0 us
  starting transfers between devices: 5.76 us -> 42.9 us
  waiting for transfers between devices: 87.2 us -> 58.4 us
  between operations: 14.6 us -> 1.22 us
  Pallas kernels: 0 us -> 8.04 us
  local copies, waits for them, and re-layouts: 19.8 us -> 24.7 us
  other arithmetic: 10.1 us -> 12.9 us
    all_gather x4 -> x0, blocking collectives: 47.9 us -> none  [the longest x1 31.1 us: shards(): lax.all_gather(group_turn, 'ep', axis=0, tiled=True)]
    ppermute x0 -> x25, waiting for transfers between devices: none -> 41.3 us  [the longest x21 25.5 us: swap_tp(): return lax.ppermute(entries, 'tp', [(i, i ^ distance) for i in range(size)])]
    all_to_all x1 -> x0, blocking collectives: 32.8 us -> none  [shards(): lax.all_to_all(outgoing, 'ep', split_axis=0, concat_axis=0, tiled=True)]
    all_gather x3 -> x0, waiting for transfers between devices: 26.7 us -> none  [the longest x1 26.7 us: shards(): lax.all_gather(received, 'tp', axis=0, tiled=True)]
    unnamed x7 -> x0, waiting for transfers between devices: 26.6 us -> none
    ppermute x0 -> x25, starting transfers between devices: none -> 24.2 us  [the longest x21 14.7 us: swap_tp(): return lax.ppermute(entries, 'tp', [(i, i ^ distance) for i in range(size)])]
    reduce_scatter x2 -> x0, waiting for transfers between devices: 13.7 us -> none  [the longest x1 13.7 us: shards(): lax.psum_scatter(mixer_term.astype(jnp.bfloat16), 'tp', scatter_dimension...]
    all_to_all x1 -> x3, starting transfers between devices: 5.52 us -> 18.7 us  [the longest x2 15 us: shards(): lax.all_to_all(summed, 'ep', split_axis=1, concat_axis=1, tiled=True)]
  transfers between devices with their start and end apart: 7 -> 28, of which waited for: 4 -> 7; matrix products, arithmetic and copies ran while one was open for 21% -> 35% of each run, Pallas kernels for 0% -> 5%
where the time goes in v1:
time: 180 us; the launch traced here: 178 us
  waiting for transfers between devices  58.4 us (32%)
  starting transfers between devices  42.9 us (24%)
  matrix products  30.2 us (17%)
  local copies, waits for them, and re-layouts  24.7 us (14%)
  other arithmetic  12.9 us (7%)
  Pallas kernels  8.04 us (4%)
    dot_general x19, matrix products, dot32(): return jnp.dot(left, right, preferred_element_type=jnp.float32)  29.7 us
    ppermute x21, waiting for transfers between devices, swap_tp(): return lax.ppermute(entries, 'tp', [(i, i ^ distance) for i in range(size)])  25.5 us
    all_to_all x2, waiting for transfers between devices, shards(): lax.all_to_all(summed, 'ep', split_axis=1, concat_axis=1, tiled=True)  17.1 us
    ppermute x4, waiting for transfers between devices, swap_ep(): return lax.ppermute(entries, 'ep', [(i, i ^ distance) for i in range(size)])  15.8 us
    all_to_all x2, starting transfers between devices, shards(): lax.all_to_all(summed, 'ep', split_axis=1, concat_axis=1, tiled=True)  15 us
    ppermute x21, starting transfers between devices, swap_tp(): return lax.ppermute(entries, 'tp', [(i, i ^ distance) for i in range(size)])  14.7 us
    unnamed x47, local copies, waits for them, and re-layouts  10.3 us
    ppermute x4, starting transfers between devices, swap_ep(): return lax.ppermute(entries, 'ep', [(i, i ^ distance) for i in range(size)])  9.52 us
  transfers between devices with their start and end apart: 28, of which 7 were waited for; matrix products, arithmetic and copies ran while one was open for 35% of the time, Pallas kernels for 5%

profile of v1, /device:TPU:0, one launch (start us, length us, event | category | flops | bytes accessed | tf_op | source)
XLA Modules:
  0.0 178.5 jit_solution(13361371108244691329)
XLA Ops:
  1.2 2.6 %collective-permute-start.11 = (bf16[128,2048]{1,0:T(8,128)(2,1)}, bf16[128,2048]{1,0:T(8,128)(2,1)}, u32[]{:S(2)}, u32[]{:S(2)}) collective-permute-start(bf16[128,2048]{1,0:T(8,128)(2,1)} %param.29), channel_id=1, source_target_pairs={{0,2},{1,3},{2,0},{3,1},{4,6},{5,7},{6,4},{7,5},{8,10},{9,11},{10,... | collective-permute-start | bytes 1572872 | tf_op jit(solution)/shard_map/ppermute | solution.py:47
  16.1 2.6 %collective-permute-start.2 = (bf16[128,288]{1,0:T(8,128)(2,1)S(1)}, bf16[128,288]{1,0:T(8,128)(2,1)S(1)}, u32[]{:S(2)}, u32[]{:S(2)}) collective-permute-start(bf16[128,288]{1,0:T(8,128)(2,1)S(1)} %pad_maximum_fusion.14), channel_id=1, source_target_pairs={{0,16},{4,20},{8,24},{12,28},{16,0},{20,4},{24,8},{28,12},{1,17},{... | collective-permute-start | bytes 221192 | tf_op jit(solution)/shard_map/ppermute | solution.py:65
  19.8 3.7 %all-to-all-start = ((bf16[2,8,16,2048]{3,2,0,1:T(8,128)(2,1)}), bf16[2,8,16,2048]{3,2,0,1:T(8,128)(2,1)S(1)}, u32[]{:S(2)}, u32[]{:S(2)}) async-start(bf16[2,8,16,2048]{3,2,0,1:T(8,128)(2,1)} %copy.93), calls=%async_computation | async-start | bytes 2097152 | tf_op jit(solution)/shard_map/all_to_all | solution.py:281
  24.4 3.7 %collective-permute-start.3 = (bf16[128,288]{1,0:T(8,128)(2,1)S(1)}, bf16[128,288]{1,0:T(8,128)(2,1)S(1)}, u32[]{:S(2)}, u32[]{:S(2)}) collective-permute-start(bf16[128,288]{1,0:T(8,128)(2,1)S(1)} %pad_maximum_fusion.14), channel_id=1, source_target_pairs={{0,24},{4,28},{8,16},{12,20},{16,8},{20,12},{24,0},{28,4},{1,25},{... | collective-permute-start | bytes 221192 | tf_op jit(solution)/shard_map/ppermute | solution.py:65
  30.4 15.8 %collective-permute-done.3 = bf16[128,288]{1,0:T(8,128)(2,1)S(1)} collective-permute-done((bf16[128,288]{1,0:T(8,128)(2,1)S(1)}, bf16[128,288]{1,0:T(8,128)(2,1)S(1)}, u32[]{:S(2)}, u32[]{:S(2)}) %collective-permute-start.3) | collective-permute-done | bytes 73760 | tf_op jit(solution)/shard_map/ppermute | solution.py:65
  49.3 7.0 %collective-permute-done.5 = bf16[512,288]{1,0:T(8,128)(2,1)} collective-permute-done((bf16[512,288]{1,0:T(8,128)(2,1)}, bf16[512,288]{1,0:T(8,128)(2,1)}, u32[]{:S(2)}, u32[]{:S(2)}) %collective-permute-start.5) | collective-permute-done | bytes 294944 | tf_op jit(solution)/shard_map/ppermute | solution.py:47
  59.1 1.8 %constant_dynamic-update-slice_fusion.6 = bf16[2048,288]{1,0:T(8,128)(2,1)} fusion(bf16[2048,288]{1,0:T(8,128)(2,1)} %get-tuple-element.49, bf16[512,288]{1,0:T(8,128)(2,1)} %collective-permute-done.4), kind=kLoop, calls=%fused_computation.134 | loop fusion | bytes 786432
  60.9 1.8 constant_dynamic-update-slice_fusion.5
  62.7 1.8 %constant_dynamic-update-slice_fusion.4.latent_ref = bf16[2048,288]{1,0:T(8,128)(2,1)} fusion(bf16[2048,288]{1,0:T(8,128)(2,1)} %constant_dynamic-update-slice_fusion.5, bf16[512,288]{1,0:T(8,128)(2,1)} %collective-permute-done.6), kind=kLoop, calls=%fused_computation.132 | loop fusion | bytes 786432 | tf_op jit(solution)/shard_map/concatenate | solution.py:284
  64.5 8.0 %attend.1 = bf16[4,64,128]{2,1,0:T(8,128)(2,1)} custom-call(bf16[4,64,128]{2,1,0:T(8,128)(2,1)} %bitcast.136, bf16[4,128,32]{2,1,0:T(8,128)(2,1)} %bitcast.135, bf16[2048,288]{1,0:T(8,128)(2,1)} %constant_dynamic-update-slice_fusion.4.latent_ref, bf16[256,512]{1,0:T(8,128)(2,1)} %key_ref.1, bf16[256,512]{1,0:T(8,128)(2,1)} %value_ref.1), custom_call_target="tpu_custom_call" | custom-call | flops 1610612736 | bytes 2097152 | tf_op jit(solution)/shard_map/attend/pallas_call | solution.py:124
  77.8 2.5 %convolution_convert_fusion.2 = bf16[256,2048]{1,0:T(8,128)(2,1)S(1)} fusion(bf16[256,2048]{1,0:T(8,128)(2,1)S(1)} %copy-done, bf16[256,2048]{1,0:T(8,128)(2,1)S(1)} %constant_dynamic-update-slice_fusion.11, bf16[2048,256]{1,0:T(8,128)(2,1)} %param.38, f32[256,256]{1,0:T(8,128)S(1)} %fusion.150), kind=kOutput, calls=%fused_computation.2 | convolution fusion | flops 537788416 | bytes 4456448 | tf_op jit(solution)/shard_map/dot_general | solution.py:26
  80.3 7.7 %collective-permute-done.13 = bf16[1,128,2048]{2,1,0:T(8,128)(2,1)} collective-permute-done((bf16[1,128,2048]{2,1,0:T(8,128)(2,1)}, bf16[1,128,2048]{2,1,0:T(8,128)(2,1)}, u32[]{:S(2)}, u32[]{:S(2)}) %collective-permute-start.13) | collective-permute-done | bytes 524320 | tf_op jit(solution)/shard_map/ppermute | solution.py:47
  92.6 3.1 %fusion.25 = f32[512,256]{1,0:T(8,128)} fusion(bf16[2,2048,256]{2,1,0:T(8,128)(2,1)} %param.34, bf16[128,2048]{1,0:T(8,128)(2,1)S(1)} %bitcast.137, bf16[128,2048]{1,0:T(8,128)(2,1)} %bitcast.28, bf16[128,2048]{1,0:T(8,128)(2,1)S(1)} %bitcast.139, bf16[128,2048]{1,0:T(8,128)(2,1)} %bitcast.26), kind=kOutput, calls=%fused_computation.49 | convolution fusion | flops 545259520 | bytes 3670016 | tf_op jit(solution)/shard_map/dot_general | solution.py:26
  95.6 4.6 %convolution_convert_fusion = bf16[512,2048]{1,0:T(8,128)(2,1)S(1)} fusion(bf16[2,256,2048]{2,1,0:T(8,128)(2,1)} %param.36, f32[512,256]{1,0:T(8,128)} %fusion.25, bf16[2,2048,256]{2,1,0:T(8,128)(2,1)} %param.35, bf16[128,2048]{1,0:T(8,128)(2,1)} %bitcast.138, bf16[128,2048]{1,0:T(8,128)(2,1)} %bitcast.28, bf16[128,2048]{1,0:T(8,128)(2,1)} %bitcast.140, ...), kind=kOutput, calls=%fused_computation | convolution fusion | flops 1083965440 | bytes 6815744 | tf_op jit(solution)/shard_map/dot_general | solution.py:26
  106.4 2.8 %fusion.30 = f32[512,256]{1,0:T(8,128)} fusion(bf16[2,2048,256]{2,1,0:T(8,128)(2,1)S(1)} %copy-done.15, bf16[128,2048]{1,0:T(8,128)(2,1)S(1)} %bitcast.141, bf16[128,2048]{1,0:T(8,128)(2,1)} %bitcast.14, bf16[128,2048]{1,0:T(8,128)(2,1)} %bitcast.13, bf16[128,2048]{1,0:T(8,128)(2,1)S(1)} %bitcast.133), kind=kOutput, calls=%fused_computation.54 | convolution fusion | flops 545259520 | bytes 3670016 | tf_op jit(solution)/shard_map/dot_general | solution.py:26
  109.2 6.0 %convolution_convert_fusion.1 = bf16[512,2048]{1,0:T(8,128)(2,1)} fusion(bf16[2,256,2048]{2,1,0:T(8,128)(2,1)} %param.36, f32[512,256]{1,0:T(8,128)} %fusion.30, bf16[2,2048,256]{2,1,0:T(8,128)(2,1)} %param.35, bf16[128,2048]{1,0:T(8,128)(2,1)} %bitcast.142, bf16[128,2048]{1,0:T(8,128)(2,1)} %bitcast.14, bf16[128,2048]{1,0:T(8,128)(2,1)} %bitcast.13, ...), kind=kOutput, calls=%fused_computation.1 | convolution fusion | flops 1083965440 | bytes 6815744 | tf_op jit(solution)/shard_map/dot_general | solution.py:26
  124.3 9.3 %collective-permute-done.23 = bf16[1,128,2048]{2,1,0:T(8,128)(2,1)S(1)} collective-permute-done((bf16[1,128,2048]{2,1,0:T(8,128)(2,1)S(1)}, bf16[1,128,2048]{2,1,0:T(8,128)(2,1)S(1)}, u32[]{:S(2)}, u32[]{:S(2)}) %collective-permute-start.23) | collective-permute-done | bytes 524320 | tf_op jit(solution)/shard_map/ppermute | solution.py:47
  134.6 11.3 %all-to-all-start.1 = ((bf16[1,8,16,2048]{3,2,0,1:T(8,128)(2,1)}), bf16[1,8,16,2048]{3,2,0,1:T(8,128)(2,1)S(1)}, u32[]{:S(2)}, u32[]{:S(2)}) async-start(bf16[1,8,16,2048]{3,2,0,1:T(8,128)(2,1)} %bitcast.37), calls=%async_computation.1 | async-start | bytes 1048576 | tf_op jit(solution)/shard_map/all_to_all | solution.py:350
  147.4 2.0 %add_convert_fusion = bf16[1,128,2048]{2,1,0:T(8,128)(2,1)} fusion(f32[1,128,2048]{2,1,0:T(8,128)S(1)} %slice_bitcast_fusion.1, bf16[1,128,2048]{2,1,0:T(8,128)(2,1)} %collective-permute-done.24), kind=kLoop, calls=%fused_computation.56 | loop fusion | flops 786432 | bytes 2097152 | tf_op jit(solution)/shard_map/convert_element_type | solution.py:348
  149.4 9.4 %all-to-all-done.1 = bf16[1,8,16,2048]{3,2,0,1:T(8,128)(2,1)S(1)} async-done(((bf16[1,8,16,2048]{3,2,0,1:T(8,128)(2,1)}), bf16[1,8,16,2048]{3,2,0,1:T(8,128)(2,1)S(1)}, u32[]{:S(2)}, u32[]{:S(2)}) %all-to-all-start.1) | async-done | bytes 524320 | tf_op jit(solution)/shard_map/all_to_all | solution.py:350
  158.8 3.7 %all-to-all-start.2 = ((bf16[1,8,16,2048]{3,2,0,1:T(8,128)(2,1)}), bf16[1,8,16,2048]{3,2,0,1:T(8,128)(2,1)S(1)}, u32[]{:S(2)}, u32[]{:S(2)}) async-start(bf16[1,8,16,2048]{3,2,0,1:T(8,128)(2,1)} %bitcast.129), calls=%async_computation.2 | async-start | bytes 1048576 | tf_op jit(solution)/shard_map/all_to_all | solution.py:350
  163.7 2.0 %fusion.4 = bf16[64,2048]{1,0:T(8,128)(2,1)} fusion(f32[64,2048]{1,0:T(8,128)S(1)} %fusion.6, bf16[128,2048]{1,0:T(8,128)(2,1)} %copy-done.7, bf16[4,64,128]{2,1,0:T(8,128)(2,1)S(1)} %copy-done.12, s32[]{:T(128)S(6)} %select_n.112), kind=kOutput, calls=%fused_computation.11 | convolution fusion | flops 34078720 | bytes 1327108 | tf_op jit(solution)/shard_map/dot_general | solution.py:26
  168.5 7.8 %all-to-all-done.2 = bf16[1,8,16,2048]{3,2,0,1:T(8,128)(2,1)S(1)} async-done(((bf16[1,8,16,2048]{3,2,0,1:T(8,128)(2,1)}), bf16[1,8,16,2048]{3,2,0,1:T(8,128)(2,1)S(1)}, u32[]{:S(2)}, u32[]{:S(2)}) %all-to-all-start.2) | async-done | bytes 524320 | tf_op jit(solution)/shard_map/all_to_all | solution.py:350
  176.5 2.0 %add_convert_fusion.1 = bf16[64,2048]{1,0:T(8,128)(2,1)} fusion(f32[64,2048]{1,0:T(8,128)S(1)} %fusion.1, f32[64,2048]{1,0:T(8,128)S(1)} %copy-done.2, bf16[64,2048]{1,0:T(8,128)(2,1)S(1)} %collective-permute-done.19, f32[64,2048]{1,0:T(8,128)} %fusion.95, bf16[128,2048]{1,0:T(8,128)(2,1)S(1)} %bitcast.126, f32[64]{0:T(128)S(1)} %get-tuple-element.56, ...), kind=kOutput, calls=%fused_computation.73 | convolution fusion | flops 34471936 | bytes 2630144 | tf_op jit(solution)/shard_map/dot_general | solution.py:26
  (153 shorter events, 54.4 us)
Async XLA Ops:
  0.6 72.0 %collective-permute-start.10 = (bf16[128,2048]{1,0:T(8,128)(2,1)}, bf16[128,2048]{1,0:T(8,128)(2,1)}, u32[]{:S(2)}, u32[]{:S(2)}) collective-permute-start(bf16[128,2048]{1,0:T(8,128)(2,1)} %param.29), channel_id=1, source_target_pairs={{0,1},{1,0},{2,3},{3,2},{4,5},{5,4},{6,7},{7,6},{8,9},{9,8},{10,11... | collective-permute-start | bytes 1572872 | tf_op jit(solution)/shard_map/ppermute | solution.py:47
  1.2 55.1 %collective-permute-start.11 = (bf16[128,2048]{1,0:T(8,128)(2,1)}, bf16[128,2048]{1,0:T(8,128)(2,1)}, u32[]{:S(2)}, u32[]{:S(2)}) collective-permute-start(bf16[128,2048]{1,0:T(8,128)(2,1)} %param.29), channel_id=1, source_target_pairs={{0,2},{1,3},{2,0},{3,1},{4,6},{5,7},{6,4},{7,5},{8,10},{9,11},{10,... | collective-permute-start | bytes 1572872 | tf_op jit(solution)/shard_map/ppermute | solution.py:47
  7.3 7.2 %collective-permute-start = (bf16[64,288]{1,0:T(8,128)(2,1)S(1)}, bf16[64,288]{1,0:T(8,128)(2,1)S(1)}, u32[]{:S(2)}, u32[]{:S(2)}) collective-permute-start(bf16[64,288]{1,0:T(8,128)(2,1)S(1)} %pad_maximum_fusion.15), channel_id=1, source_target_pairs={{0,4},{4,0},{8,12},{12,8},{16,20},{20,16},{24,28},{28,24},{1,5},{5... | collective-permute-start | bytes 110600 | tf_op jit(solution)/shard_map/ppermute | solution.py:65
  11.0 47.5 %collective-permute-start.8 = (bf16[64,2048]{1,0:T(8,128)(2,1)S(1)}, bf16[64,2048]{1,0:T(8,128)(2,1)}, u32[]{:S(2)}, u32[]{:S(2)}) collective-permute-start(bf16[64,2048]{1,0:T(8,128)(2,1)S(1)} %fusion.40), channel_id=1, source_target_pairs={{0,2},{1,3},{2,0},{3,1},{4,6},{5,7},{6,4},{7,5},{8,10},{9,11},{10,... | collective-permute-start | bytes 786440 | tf_op jit(solution)/shard_map/ppermute | solution.py:47
  14.5 9.8 %collective-permute-start.1 = (bf16[128,288]{1,0:T(8,128)(2,1)S(1)}, bf16[128,288]{1,0:T(8,128)(2,1)}, u32[]{:S(2)}, u32[]{:S(2)}) collective-permute-start(bf16[128,288]{1,0:T(8,128)(2,1)S(1)} %pad_maximum_fusion.14), channel_id=1, source_target_pairs={{0,8},{4,12},{8,0},{12,4},{16,24},{20,28},{24,16},{28,20},{1,9},{5... | collective-permute-start | bytes 221192 | tf_op jit(solution)/shard_map/ppermute | solution.py:65
  16.1 13.6 %collective-permute-start.2 = (bf16[128,288]{1,0:T(8,128)(2,1)S(1)}, bf16[128,288]{1,0:T(8,128)(2,1)S(1)}, u32[]{:S(2)}, u32[]{:S(2)}) collective-permute-start(bf16[128,288]{1,0:T(8,128)(2,1)S(1)} %pad_maximum_fusion.14), channel_id=1, source_target_pairs={{0,16},{4,20},{8,24},{12,28},{16,0},{20,4},{24,8},{28,12},{1,17},{... | collective-permute-start | bytes 221192 | tf_op jit(solution)/shard_map/ppermute | solution.py:65
  19.8 52.7 %all-to-all-start = ((bf16[2,8,16,2048]{3,2,0,1:T(8,128)(2,1)}), bf16[2,8,16,2048]{3,2,0,1:T(8,128)(2,1)S(1)}, u32[]{:S(2)}, u32[]{:S(2)}) async-start(bf16[2,8,16,2048]{3,2,0,1:T(8,128)(2,1)} %copy.93), calls=%async_computation | async-start | bytes 2097152 | tf_op jit(solution)/shard_map/all_to_all | solution.py:281
  24.4 21.8 %collective-permute-start.3 = (bf16[128,288]{1,0:T(8,128)(2,1)S(1)}, bf16[128,288]{1,0:T(8,128)(2,1)S(1)}, u32[]{:S(2)}, u32[]{:S(2)}) collective-permute-start(bf16[128,288]{1,0:T(8,128)(2,1)S(1)} %pad_maximum_fusion.14), channel_id=1, source_target_pairs={{0,24},{4,28},{8,16},{12,20},{16,8},{20,12},{24,0},{28,4},{1,25},{... | collective-permute-start | bytes 221192 | tf_op jit(solution)/shard_map/ppermute | solution.py:65
  46.9 9.4 %collective-permute-start.5 = (bf16[512,288]{1,0:T(8,128)(2,1)}, bf16[512,288]{1,0:T(8,128)(2,1)}, u32[]{:S(2)}, u32[]{:S(2)}) collective-permute-start(bf16[512,288]{1,0:T(8,128)(2,1)} %get-tuple-element.48), channel_id=1, source_target_pairs={{0,2},{1,3},{2,0},{3,1},{4,6},{5,7},{6,4},{7,5},{8,10},{9,11},{10,... | collective-permute-start | bytes 884744 | tf_op jit(solution)/shard_map/ppermute | solution.py:47
  48.7 9.9 %collective-permute-start.4 = (bf16[512,288]{1,0:T(8,128)(2,1)}, bf16[512,288]{1,0:T(8,128)(2,1)}, u32[]{:S(2)}, u32[]{:S(2)}) collective-permute-start(bf16[512,288]{1,0:T(8,128)(2,1)} %get-tuple-element.48), channel_id=1, source_target_pairs={{0,1},{1,0},{2,3},{3,2},{4,5},{5,4},{6,7},{7,6},{8,9},{9,8},{10,11... | collective-permute-start | bytes 884744 | tf_op jit(solution)/shard_map/ppermute | solution.py:47
  56.3 6.4 %collective-permute-start.6 = (bf16[512,288]{1,0:T(8,128)(2,1)}, bf16[512,288]{1,0:T(8,128)(2,1)}, u32[]{:S(2)}, u32[]{:S(2)}) collective-permute-start(bf16[512,288]{1,0:T(8,128)(2,1)} %collective-permute-done.5), channel_id=1, source_target_pairs={{0,1},{1,0},{2,3},{3,2},{4,5},{5,4},{6,7},{7,6},{8,9},{9,8},{10,11... | collective-permute-start | bytes 884744 | tf_op jit(solution)/shard_map/ppermute | solution.py:47
  56.3 16.4 %collective-permute-start.12 = (bf16[128,2048]{1,0:T(8,128)(2,1)}, bf16[128,2048]{1,0:T(8,128)(2,1)S(1)}, u32[]{:S(2)}, u32[]{:S(2)}) collective-permute-start(bf16[128,2048]{1,0:T(8,128)(2,1)} %collective-permute-done.11), channel_id=1, source_target_pairs={{0,1},{1,0},{2,3},{3,2},{4,5},{5,4},{6,7},{7,6},{8,9},{9,8},{10,11... | collective-permute-start | bytes 1572872 | tf_op jit(solution)/shard_map/ppermute | solution.py:47
  58.6 14.0 %collective-permute-start.7 = (bf16[64,2048]{1,0:T(8,128)(2,1)S(1)}, bf16[64,2048]{1,0:T(8,128)(2,1)S(1)}, u32[]{:S(2)}, u32[]{:S(2)}) collective-permute-start(bf16[64,2048]{1,0:T(8,128)(2,1)S(1)} %fusion.40), channel_id=1, source_target_pairs={{0,1},{1,0},{2,3},{3,2},{4,5},{5,4},{6,7},{7,6},{8,9},{9,8},{10,11... | collective-permute-start | bytes 786440 | tf_op jit(solution)/shard_map/ppermute | solution.py:47
  58.6 14.0 %collective-permute-start.9 = (bf16[64,2048]{1,0:T(8,128)(2,1)}, bf16[64,2048]{1,0:T(8,128)(2,1)}, u32[]{:S(2)}, u32[]{:S(2)}) collective-permute-start(bf16[64,2048]{1,0:T(8,128)(2,1)} %collective-permute-done.8), channel_id=1, source_target_pairs={{0,1},{1,0},{2,3},{3,2},{4,5},{5,4},{6,7},{7,6},{8,9},{9,8},{10,11... | collective-permute-start | bytes 786440 | tf_op jit(solution)/shard_map/ppermute | solution.py:47
  73.8 14.2 %collective-permute-start.13 = (bf16[1,128,2048]{2,1,0:T(8,128)(2,1)}, bf16[1,128,2048]{2,1,0:T(8,128)(2,1)}, u32[]{:S(2)}, u32[]{:S(2)}) collective-permute-start(bf16[1,128,2048]{2,1,0:T(8,128)(2,1)} %get-tuple-element.40), channel_id=1, source_target_pairs={{0,2},{1,3},{2,0},{3,1},{4,6},{5,7},{6,4},{7,5},{8,10},{9,11},{10,... | collective-permute-start | bytes 1572872 | tf_op jit(solution)/shard_map/ppermute | solution.py:47
  88.6 14.2 %collective-permute-start.15 = (bf16[1,128,2048]{2,1,0:T(8,128)(2,1)}, bf16[1,128,2048]{2,1,0:T(8,128)(2,1)}, u32[]{:S(2)}, u32[]{:S(2)}) collective-permute-start(bf16[1,128,2048]{2,1,0:T(8,128)(2,1)} %get-tuple-element.36), channel_id=1, source_target_pairs={{0,2},{1,3},{2,0},{3,1},{4,6},{5,7},{6,4},{7,5},{8,10},{9,11},{10,... | collective-permute-start | bytes 1572872 | tf_op jit(solution)/shard_map/ppermute | solution.py:47
  90.2 15.4 %collective-permute-start.14 = (bf16[1,128,2048]{2,1,0:T(8,128)(2,1)}, bf16[1,128,2048]{2,1,0:T(8,128)(2,1)}, u32[]{:S(2)}, u32[]{:S(2)}) collective-permute-start(bf16[1,128,2048]{2,1,0:T(8,128)(2,1)} %get-tuple-element.36), channel_id=1, source_target_pairs={{0,1},{1,0},{2,3},{3,2},{4,5},{5,4},{6,7},{7,6},{8,9},{9,8},{10,11... | collective-permute-start | bytes 1572872 | tf_op jit(solution)/shard_map/ppermute | solution.py:47
  91.1 11.8 %collective-permute-start.18 = (bf16[2,64,2048]{2,1,0:T(8,128)(2,1)}, bf16[2,64,2048]{2,1,0:T(8,128)(2,1)}, u32[]{:S(2)}, u32[]{:S(2)}) collective-permute-start(bf16[2,64,2048]{2,1,0:T(8,128)(2,1)} %slice.99), channel_id=1, source_target_pairs={{0,1},{1,0},{2,3},{3,2},{4,5},{5,4},{6,7},{7,6},{8,9},{9,8},{10,11... | collective-permute-start | bytes 1572872 | tf_op jit(solution)/shard_map/ppermute | solution.py:47
  101.4 15.7 %collective-permute-start.22 = (bf16[2,1,128,2048]{3,2,0,1:T(8,128)(2,1)}, bf16[2,1,128,2048]{3,2,0,1:T(8,128)(2,1)}, u32[]{:S(2)}, u32[]{:S(2)}) collective-permute-start(bf16[2,1,128,2048]{3,2,0,1:T(8,128)(2,1)} %slice.108), channel_id=1, source_target_pairs={{0,1},{1,0},{2,3},{3,2},{4,5},{5,4},{6,7},{7,6},{8,9},{9,8},{10,11... | collective-permute-start | bytes 3145736 | tf_op jit(solution)/shard_map/ppermute | solution.py:47
  118.8 14.9 %collective-permute-start.23 = (bf16[1,128,2048]{2,1,0:T(8,128)(2,1)S(1)}, bf16[1,128,2048]{2,1,0:T(8,128)(2,1)S(1)}, u32[]{:S(2)}, u32[]{:S(2)}) collective-permute-start(bf16[1,128,2048]{2,1,0:T(8,128)(2,1)S(1)} %fusion.42), channel_id=1, source_target_pairs={{0,2},{1,3},{2,0},{3,1},{4,6},{5,7},{6,4},{7,5},{8,10},{9,11},{10,... | collective-permute-start | bytes 1572872 | tf_op jit(solution)/shard_map/ppermute | solution.py:47
  123.7 23.7 %collective-permute-start.24 = (bf16[1,128,2048]{2,1,0:T(8,128)(2,1)}, bf16[1,128,2048]{2,1,0:T(8,128)(2,1)}, u32[]{:S(2)}, u32[]{:S(2)}) collective-permute-start(bf16[1,128,2048]{2,1,0:T(8,128)(2,1)} %fusion.41), channel_id=1, source_target_pairs={{0,2},{1,3},{2,0},{3,1},{4,6},{5,7},{6,4},{7,5},{8,10},{9,11},{10,... | collective-permute-start | bytes 1572872 | tf_op jit(solution)/shard_map/ppermute | solution.py:47
  134.6 24.2 %all-to-all-start.1 = ((bf16[1,8,16,2048]{3,2,0,1:T(8,128)(2,1)}), bf16[1,8,16,2048]{3,2,0,1:T(8,128)(2,1)S(1)}, u32[]{:S(2)}, u32[]{:S(2)}) async-start(bf16[1,8,16,2048]{3,2,0,1:T(8,128)(2,1)} %bitcast.37), calls=%async_computation.1 | async-start | bytes 1048576 | tf_op jit(solution)/shard_map/all_to_all | solution.py:350
  158.8 17.5 %all-to-all-start.2 = ((bf16[1,8,16,2048]{3,2,0,1:T(8,128)(2,1)}), bf16[1,8,16,2048]{3,2,0,1:T(8,128)(2,1)S(1)}, u32[]{:S(2)}, u32[]{:S(2)}) async-start(bf16[1,8,16,2048]{3,2,0,1:T(8,128)(2,1)} %bitcast.129), calls=%async_computation.2 | async-start | bytes 1048576 | tf_op jit(solution)/shard_map/all_to_all | solution.py:350
  165.7 10.8 %collective-permute-start.19 = (bf16[64,2048]{1,0:T(8,128)(2,1)}, bf16[64,2048]{1,0:T(8,128)(2,1)S(1)}, u32[]{:S(2)}, u32[]{:S(2)}) collective-permute-start(bf16[64,2048]{1,0:T(8,128)(2,1)} %fusion.51), channel_id=1, source_target_pairs={{0,2},{1,3},{2,0},{3,1},{4,6},{5,7},{6,4},{7,5},{8,10},{9,11},{10,... | collective-permute-start | bytes 786440 | tf_op jit(solution)/shard_map/ppermute | solution.py:47
  (23 other events, 297.2 us)
